TPU v7x, 32 devices: a whole 2x2x4 slice. The times are simulated.
32 devices in a mesh: kv: 8 (over z, y), tp: 4 (over x, core).
Axes of the slice: x: 2, y: 2, z: 4, core: 2. Of those that a mesh axis runs over, the one named last changes fastest.
Arguments:
- tokens: bfloat16 [128, 4096], P(None, ('kv', 'tp')), may hold values from -64 to 64
- mix_gain: float32 [4096], P('kv'), may hold values from 0.1 to 1.9
- w_query: bfloat16 [4096, 3072], P('kv', 'tp'), may hold values from -0.09375 to 0.09375
- w_key: bfloat16 [4096, 3072], P('kv', 'tp'), may hold values from -0.09375 to 0.09375
- w_value: bfloat16 [4096, 3072], P('kv', 'tp'), may hold values from -0.09375 to 0.09375
- w_gate: bfloat16 [4096, 3072], P('kv', 'tp'), may hold values from -0.09375 to 0.09375
- w_beta: bfloat16 [4096, 24], P('kv'), may hold values from -0.09375 to 0.09375
- w_decay: bfloat16 [4096, 24], P('kv'), may hold values from -0.09375 to 0.09375
- decay_rate: float32 [24], P('tp'), may hold values from 0.15 to 1.5
- out_gain: float32 [128], replicated, may hold values from 0.1 to 1.9
- state: float32 [128, 24, 128, 128], P('kv', 'tp'), may hold values from -0.6 to 0.6
- w_out: bfloat16 [3072, 4096], P('tp', 'kv'), may hold values from -0.109375 to 0.109375
- mlp_gain: float32 [4096], replicated, may hold values from 0.1 to 1.9
- w_up: bfloat16 [4096, 16384], P(None, ('kv', 'tp')), may hold values from -0.09375 to 0.09375
- w_down: bfloat16 [16384, 4096], P(('kv', 'tp')), may hold values from -0.09375 to 0.09375
Outputs:
- mixed: bfloat16 [128, 4096], P(None, ('kv', 'tp'))
- new_state: float32 [128, 24, 128, 128], P('kv', 'tp')
All inputs are finite; a program needn't handle non-finite values.
Results may differ from a plain program's by a relative error of at most 0.0063.
Values may be sent and summed in bfloat16 or wider, within the bound.
A program may use at most 64 MiB of HBM per device.

v0:
```python
import jax
import jax.numpy as jnp
from jax import lax
from jax.sharding import PartitionSpec as P

D = 4096
EPSILON = 1e-06


def head_norm(values):
    return values * lax.rsqrt(jnp.sum(values * values, axis=-1, keepdims=True) + EPSILON)


def feed_forward(segment, mlp_gain, w_up, w_down):
    segment_f = segment.astype(jnp.float32)
    normed_mlp = (
        segment_f
        * lax.rsqrt(jnp.mean(segment_f * segment_f, axis=1, keepdims=True) + EPSILON)
        * mlp_gain[None, :]
    ).astype(jnp.bfloat16)
    hidden = jnp.square(
        jax.nn.relu(jnp.dot(normed_mlp, w_up, preferred_element_type=jnp.float32))
    ).astype(jnp.bfloat16)
    return jnp.dot(hidden, w_down, preferred_element_type=jnp.float32)


def local(
    tokens,
    mix_gain,
    w_query,
    w_key,
    w_value,
    w_gate,
    w_beta,
    w_decay,
    decay_rate,
    out_gain,
    state,
    w_out,
    mlp_gain,
    w_up,
    w_down,
):
    local_rows = state.shape[0]
    local_heads = decay_rate.shape[0]
    head_size = state.shape[2]
    all_heads = w_beta.shape[1]
    columns = lax.all_gather(tokens, "tp", axis=1, tiled=True)
    columns_f = columns.astype(jnp.float32)
    normed = (columns_f * mix_gain[None, :]).astype(jnp.bfloat16)
    part_query = jnp.dot(normed, w_query, preferred_element_type=jnp.float32)
    part_key = jnp.dot(normed, w_key, preferred_element_type=jnp.float32)
    part_value = jnp.dot(normed, w_value, preferred_element_type=jnp.float32)
    part_gate = jnp.dot(normed, w_gate, preferred_element_type=jnp.float32)
    part_rates = jnp.dot(
        normed, jnp.concatenate([w_beta, w_decay], axis=1), preferred_element_type=jnp.float32
    )
    summed = (
        lax.psum_scatter(part_query, "kv", scatter_dimension=0, tiled=True),
        lax.psum_scatter(part_key, "kv", scatter_dimension=0, tiled=True),
        lax.psum_scatter(part_value, "kv", scatter_dimension=0, tiled=True),
        lax.psum_scatter(part_gate, "kv", scatter_dimension=0, tiled=True),
        lax.psum_scatter(part_rates, "kv", scatter_dimension=0, tiled=True),
        lax.psum_scatter(
            jnp.sum(columns_f * columns_f, axis=1), "kv", scatter_dimension=0, tiled=True
        ),
    )
    own_squares = summed[5]
    row_scale = lax.rsqrt(own_squares / D + EPSILON)[:, None]
    shape_heads = (local_rows, local_heads, head_size)
    query = head_norm(jax.nn.silu((summed[0] * row_scale).reshape(shape_heads))) * head_size ** (
        -0.5
    )
    key = head_norm(jax.nn.silu((summed[1] * row_scale).reshape(shape_heads)))
    value = jax.nn.silu((summed[2] * row_scale).reshape(shape_heads))
    gate_raw = (summed[3] * row_scale).reshape(shape_heads)
    rates = summed[4] * row_scale
    head_start = lax.axis_index("tp") * local_heads
    beta = jax.nn.sigmoid(lax.dynamic_slice_in_dim(rates, head_start, local_heads, 1))
    decay_raw = lax.dynamic_slice_in_dim(rates, all_heads + head_start, local_heads, 1)
    decay = jnp.exp(-decay_rate[None, :] * jax.nn.softplus(decay_raw))
    faded = state * decay[:, :, None, None]
    recalled = jnp.einsum("bhkv,bhk->bhv", faded, key, precision=lax.Precision.HIGHEST)
    change = beta[:, :, None] * (value - recalled)
    new_state = faded + key[:, :, :, None] * change[:, :, None, :]
    readout = jnp.einsum("bhkv,bhk->bhv", new_state, query, precision=lax.Precision.HIGHEST)
    scaled = (
        readout
        * lax.rsqrt(jnp.mean(readout * readout, axis=-1, keepdims=True) + EPSILON)
        * out_gain
    )
    merged = (
        (scaled * jax.nn.silu(gate_raw))
        .reshape(local_rows, local_heads * head_size)
        .astype(jnp.bfloat16)
    )
    partial_out = jnp.dot(
        lax.all_gather(merged, "kv", axis=0, tiled=True), w_out, preferred_element_type=jnp.float32
    )
    branch_sum = lax.psum_scatter(partial_out, "tp", scatter_dimension=1, tiled=True)
    residual = (tokens.astype(jnp.float32) + branch_sum).astype(jnp.bfloat16)
    whole_rows = lax.all_gather(residual, ("kv", "tp"), axis=1, tiled=True)
    partial_mlp = feed_forward(whole_rows, mlp_gain, w_up, w_down)
    branch = lax.psum_scatter(partial_mlp, ("kv", "tp"), scatter_dimension=1, tiled=True)
    mixed = (residual.astype(jnp.float32) + branch).astype(jnp.bfloat16)
    return (mixed, new_state)


def solution(mesh):
    placed = (
        P(None, ("kv", "tp")),
        P("kv"),
        P("kv", "tp"),
        P("kv", "tp"),
        P("kv", "tp"),
        P("kv", "tp"),
        P("kv", None),
        P("kv", None),
        P("tp"),
        P(),
        P("kv", "tp", None, None),
        P("tp", "kv"),
        P(),
        P(None, ("kv", "tp")),
        P(("kv", "tp"), None),
    )
    return jax.shard_map(
        local,
        mesh=mesh,
        in_specs=placed,
        out_specs=(P(None, ("kv", "tp")), P("kv", "tp", None, None)),
        check_vma=False,
    )
```

profile of v0, /device:TPU:0, one launch (start us, length us, event | category | flops | bytes accessed | tf_op | source)
XLA Modules:
  0.0 618.0 jit_solution(8560261450145057802)
XLA Ops:
  7.3 6.9 %all_gather.9 = bf16[128,512]{1,0:T(8,128)(2,1)S(1)} all-gather(bf16[128,128]{1,0:T(8,128)(2,1)} %param.15), channel_id=1, replica_groups=mesh['kv'=8,'tp'=4] {'tp'}, dimensions={1}, use_global_device_ids=true | all-gather | bytes 163840 | tf_op jit(solution)/shard_map/all_gather | solution.py:48
  14.2 1.6 fusion.31
  15.8 1.7 fusion.29
  17.6 2.2 fusion.27
  19.8 1.7 fusion.25
  21.6 1.0 fusion.23
  24.1 22.1 %all-reduce = f32[128]{0:T(128)S(1)} all-reduce(f32[128]{0:T(128)S(1)} %fusion.16), channel_id=3, replica_groups=mesh['kv'=8,'tp'=4] {'kv'}, use_global_device_ids=true, to_apply=%region_2.0.clone | all-reduce | flops 128 | bytes 1024
  46.3 33.7 %reduce-scatter.8.cloned.1.call-done = f32[16,48]{1,0:T(8,128)} async-done(((f32[128,48]{1,0:T(8,128)}), f32[16,48]{1,0:T(8,128)}) %reduce-scatter.8.cloned.1.call-update) | async-done | bytes 3088 | tf_op jit(solution)/shard_map/reduce_scatter | solution.py:63
  80.9 63.6 %reduce-scatter.10.cloned.1.call-done = f32[16,768]{1,0:T(8,128)} async-done(((f32[128,768]{1,0:T(8,128)}), f32[16,768]{1,0:T(8,128)}) %reduce-scatter.10.cloned.1.call-update) | async-done | bytes 49168 | tf_op jit(solution)/shard_map/reduce_scatter | solution.py:60
  144.5 64.5 %reduce-scatter.12.cloned.1.call-done = f32[16,768]{1,0:T(8,128)} async-done(((f32[128,768]{1,0:T(8,128)}), f32[16,768]{1,0:T(8,128)}) %reduce-scatter.12.cloned.1.call-update) | async-done | bytes 49168 | tf_op jit(solution)/shard_map/reduce_scatter | solution.py:61
  209.0 64.3 %reduce-scatter.14.cloned.1.call-done = f32[16,768]{1,0:T(8,128)} async-done(((f32[128,768]{1,0:T(8,128)}), f32[16,768]{1,0:T(8,128)}) %reduce-scatter.14.cloned.1.call-update) | async-done | bytes 49168 | tf_op jit(solution)/shard_map/reduce_scatter | solution.py:59
  273.3 64.9 %reduce-scatter.16.cloned.1.call-done = f32[16,768]{1,0:T(8,128)} async-done(((f32[128,768]{1,0:T(8,128)}), f32[16,768]{1,0:T(8,128)}) %reduce-scatter.16.cloned.1.call-update) | async-done | bytes 49168 | tf_op jit(solution)/shard_map/reduce_scatter | solution.py:62
  339.7 7.7 %fusion = f32[16,6,1,128]{3,2,1,0:T(1,128)S(1)} fusion(f32[16,6,128,128]{3,2,1,0:T(8,128)} %param.25, f32[16,6]{1,0:T(8,128)S(1)} %get-tuple-element.3, f32[16,6,128,1]{2,1,0,3:T(8,128)S(1)} %fusion.55), kind=kOutput, calls=%fused_computation.1 | convolution fusion | flops 20447232 | bytes 6390144 | tf_op jit(solution)/shard_map/bhkv,bhk->bhv/dot_general | solution.py:83
  347.6 4.5 multiply_add_fusion
  352.1 2.7 copy-done.1
  354.8 5.4 fusion.36
  360.4 30.7 %all_gather.10 = bf16[128,768]{1,0:T(8,128)(2,1)S(1)} all-gather(bf16[16,768]{1,0:T(8,128)(2,1)S(1)} %bitcast.34), channel_id=1, replica_groups=mesh['kv'=8,'tp'=4] {'kv'}, dimensions={0}, use_global_device_ids=true | all-gather | bytes 221184 | tf_op jit(solution)/shard_map/all_gather | solution.py:98
  392.2 19.3 %reduce-scatter.18.cloned.1.call-done = f32[128,128]{1,0:T(8,128)} async-done(((f32[128,512]{1,0:T(8,128)}), f32[128,128]{1,0:T(8,128)}) %reduce-scatter.18.cloned.1.call-update) | async-done | bytes 65552 | tf_op jit(solution)/shard_map/reduce_scatter | solution.py:100
  411.5 1.5 add_convert_fusion.1
  413.0 50.4 %all-gather.2.cloned.1.call-done = bf16[128,4096]{1,0:T(8,128)(2,1)} async-done(((bf16[128,128]{1,0:T(8,128)(2,1)}), bf16[128,4096]{1,0:T(8,128)(2,1)}) %all-gather.2.cloned.1.call-update) | async-done | bytes 1048592 | tf_op jit(solution)/shard_map/all_gather | solution.py:102
  463.4 1.5 fusion.3
  464.9 6.6 %fusion.8 = f32[128,4096]{1,0:T(8,128)} fusion(bf16[512,4096]{1,0:T(8,128)(2,1)} %param.29, bf16[4096,512]{1,0:T(8,128)(2,1)} %param.28, bf16[128,4096]{1,0:T(8,128)(2,1)} %all-gather.2.cloned.1.call-done, f32[4096]{0:T(1024)S(1)} %copy-done.8, f32[128]{0:T(128)S(1)} %add_rsqrt_fusion.3), kind=kOutput, calls=%fused_computation.12 | convolution fusion | flops 1076035584 | bytes 11551232 | tf_op jit(solution)/shard_map/dot_general | solution.py:24
  471.5 138.2 %reduce-scatter.20.cloned.1.call-done = f32[128,128]{1,0:T(8,128)} async-done(((f32[128,4096]{1,0:T(8,128)}), f32[128,128]{1,0:T(8,128)}) %reduce-scatter.20.cloned.1.call-update) | async-done | bytes 65552 | tf_op jit(solution)/shard_map/reduce_scatter | solution.py:104
  609.7 1.5 add_convert_fusion
  (64 shorter events, 4.9 us)
Async XLA Ops:
  7.2 8.6 %copy-start = (bf16[512,768]{1,0:T(8,128)(2,1)S(1)}, bf16[512,768]{1,0:T(8,128)(2,1)}, u32[]{:S(2)}) copy-start(bf16[512,768]{1,0:T(8,128)(2,1)} %param.18) | copy-start | bytes 2359300
  7.2 15.6 %copy-start.11 = (u32[32]{0:T(128)S(1)}, u32[32]{0:T(128)}, u32[]{:S(2)}) copy-start(u32[32]{0:T(128)} %constant.45) | copy-start | bytes 388
  7.2 14.4 %copy-start.7 = (f32[512]{0:T(512)S(1)}, f32[512]{0:T(512)}, u32[]{:S(2)}) copy-start(f32[512]{0:T(512)} %param.16) | copy-start | bytes 6148
  7.2 12.6 %copy-start.2 = (bf16[512,768]{1,0:T(8,128)(2,1)S(1)}, bf16[512,768]{1,0:T(8,128)(2,1)}, u32[]{:S(2)}) copy-start(bf16[512,768]{1,0:T(8,128)(2,1)} %param.17) | copy-start | bytes 2359300
  7.2 14.4 %copy-start.3 = (bf16[512,768]{1,0:T(8,128)(2,1)S(1)}, bf16[512,768]{1,0:T(8,128)(2,1)}, u32[]{:S(2)}) copy-start(bf16[512,768]{1,0:T(8,128)(2,1)} %param.20) | copy-start | bytes 2359300
  7.2 15.5 %copy-start.10 = (f32[6]{0:T(128)S(1)}, f32[6]{0:T(128)}, u32[]{:S(2)}) copy-start(f32[6]{0:T(128)} %param.23) | copy-start | bytes 76
  7.2 72.8 %reduce-scatter.8.cloned.1.call-start = ((), (), s32[]{:S(2)}) async-start(), calls=%async_computation.7 | async-start | bytes 73728 | tf_op jit(solution)/shard_map/reduce_scatter | solution.py:63
  15.8 128.7 %reduce-scatter.10.cloned.1.call-start = ((), (), s32[]{:S(2)}) async-start(), calls=%async_computation.8 | async-start | bytes 442368 | tf_op jit(solution)/shard_map/reduce_scatter | solution.py:60
  17.5 191.4 %reduce-scatter.12.cloned.1.call-start = ((), (), s32[]{:S(2)}) async-start(), calls=%async_computation.9 | async-start | bytes 442368 | tf_op jit(solution)/shard_map/reduce_scatter | solution.py:61
  19.8 253.5 %reduce-scatter.14.cloned.1.call-start = ((), (), s32[]{:S(2)}) async-start(), calls=%async_computation.10 | async-start | bytes 442368 | tf_op jit(solution)/shard_map/reduce_scatter | solution.py:59
  21.6 316.6 %reduce-scatter.16.cloned.1.call-start = ((), (), s32[]{:S(2)}) async-start(), calls=%async_computation.11 | async-start | bytes 442368 | tf_op jit(solution)/shard_map/reduce_scatter | solution.py:62
  22.7 388.8 %reduce-scatter.18.cloned.1.call-start = ((), (), s32[]{:S(2)}) async-start(), calls=%async_computation.12 | async-start | bytes 327680 | tf_op jit(solution)/shard_map/reduce_scatter | solution.py:100
  352.1 2.7 copy-start.1
  354.8 5.6 copy-start.9
  354.8 36.4 %copy-start.4 = (bf16[768,512]{1,0:T(8,128)(2,1)S(1)}, bf16[768,512]{1,0:T(8,128)(2,1)}, u32[]{:S(2)}) copy-start(bf16[768,512]{1,0:T(8,128)(2,1)} %param.26) | copy-start | bytes 2359300
  354.8 56.7 %copy-start.6 = (bf16[128,128]{1,0:T(8,128)(2,1)S(1)}, bf16[128,128]{1,0:T(8,128)(2,1)}, u32[]{:S(2)}) copy-start(bf16[128,128]{1,0:T(8,128)(2,1)} %param.15) | copy-start | bytes 98308
  354.8 110.1 %copy-start.8 = (f32[4096]{0:T(1024)S(1)}, f32[4096]{0:T(1024)}, u32[]{:S(2)}) copy-start(f32[4096]{0:T(1024)} %param.27) | copy-start | bytes 49156
  392.2 71.2 %all-gather.2.cloned.1.call-start = ((), (), s32[]{:S(2)}) async-start(), calls=%async_computation.13 | async-start | bytes 1081344 | tf_op jit(solution)/shard_map/all_gather | solution.py:102
  413.0 196.7 %reduce-scatter.20.cloned.1.call-start = ((), (), s32[]{:S(2)}) async-start(), calls=%async_computation.14 | async-start | bytes 2162688 | tf_op jit(solution)/shard_map/reduce_scatter | solution.py:104
  464.9 144.8 %copy-start.5 = (bf16[128,128]{1,0:T(8,128)(2,1)S(1)}, bf16[128,128]{1,0:T(8,128)(2,1)}, u32[]{:S(2)}) copy-start(bf16[128,128]{1,0:T(8,128)(2,1)} %add_convert_fusion.1) | copy-start | bytes 98308
Sparse Core Ops, SparseCore 0:
  15.9 64.0 reduce-scatter.7
  83.3 61.1 reduce-scatter.9
  147.8 61.1 reduce-scatter.11
  212.1 61.1 reduce-scatter.13
  277.0 61.1 reduce-scatter.15
  392.3 19.1 reduce-scatter.17
  414.9 48.4 all-gather.1
  471.6 138.0 reduce-scatter.19
where the time goes:
time: 619 us; the launch traced here: 618 us
  waiting for transfers between devices  499 us (81%)
  blocking collectives  59.7 us (10%)
  matrix products  28.8 us (5%)
  between operations  15.1 us (2%)
  other arithmetic  11.7 us (2%)
    reduce_scatter x1, waiting for transfers between devices, local(): lax.psum_scatter(partial_mlp, ('kv', 'tp'), scatter_dimension=1, tiled=True)  138 us
    reduce_scatter x1, waiting for transfers between devices, local(): lax.psum_scatter(part_gate, 'kv', scatter_dimension=0, tiled=True)  64.9 us
    reduce_scatter x1, waiting for transfers between devices, local(): lax.psum_scatter(part_value, 'kv', scatter_dimension=0, tiled=True)  64.5 us
    reduce_scatter x1, waiting for transfers between devices, local(): lax.psum_scatter(part_query, 'kv', scatter_dimension=0, tiled=True)  64.3 us
    reduce_scatter x1, waiting for transfers between devices, local(): lax.psum_scatter(part_key, 'kv', scatter_dimension=0, tiled=True)  63.6 us
    all_gather x1, waiting for transfers between devices, local(): whole_rows = lax.all_gather(residual, ('kv', 'tp'), axis=1, tiled=True)  50.4 us
    reduce_scatter x1, waiting for transfers between devices, local(): lax.psum_scatter(part_rates, 'kv', scatter_dimension=0, tiled=True)  33.7 us
    all_gather x1, blocking collectives, local(): lax.all_gather(merged, 'kv', axis=0, tiled=True)  30.7 us
  transfers between devices with their start and end apart: 8, of which 8 were waited for; matrix products, arithmetic and copies ran while one was open for 1% of the time, Pallas kernels for 0%

commit v1 on v0

--- a/solution.py
+++ b/solution.py
@@ -99,7 +99,7 @@
     )
     branch_sum = lax.psum_scatter(partial_out, "tp", scatter_dimension=1, tiled=True)
     residual = (tokens.astype(jnp.float32) + branch_sum).astype(jnp.bfloat16)
-    whole_rows = lax.all_gather(residual, ("kv", "tp"), axis=1, tiled=True)
+    whole_rows = jnp.concatenate(lax.all_gather(residual, ("kv", "tp")), axis=1)
     partial_mlp = feed_forward(whole_rows, mlp_gain, w_up, w_down)
     branch = lax.psum_scatter(partial_mlp, ("kv", "tp"), scatter_dimension=1, tiled=True)
     mixed = (residual.astype(jnp.float32) + branch).astype(jnp.bfloat16)

time: 619 us -> 630 us (1.018)
  no operation moved by 1% of the time
where the time goes in v1:
time: 630 us; the launch traced here: 629 us
  waiting for transfers between devices  503 us (80%)
  blocking collectives  59.7 us (9%)
  matrix products  28.8 us (5%)
  other arithmetic  16.2 us (3%)
  between operations  15.1 us (2%)
    reduce_scatter x1, waiting for transfers between devices, local(): lax.psum_scatter(partial_mlp, ('kv', 'tp'), scatter_dimension=1, tiled=True)  138 us
    reduce_scatter x1, waiting for transfers between devices, local(): lax.psum_scatter(part_gate, 'kv', scatter_dimension=0, tiled=True)  64.9 us
    reduce_scatter x1, waiting for transfers between devices, local(): lax.psum_scatter(part_value, 'kv', scatter_dimension=0, tiled=True)  64.5 us
    reduce_scatter x1, waiting for transfers between devices, local(): lax.psum_scatter(part_query, 'kv', scatter_dimension=0, tiled=True)  64.3 us
    reduce_scatter x1, waiting for transfers between devices, local(): lax.psum_scatter(part_key, 'kv', scatter_dimension=0, tiled=True)  63.6 us
    all_gather x1, waiting for transfers between devices, local(): whole_rows = jnp.concatenate(lax.all_gather(residual, ('kv', 'tp')), axis=1)  55.4 us
    reduce_scatter x1, waiting for transfers between devices, local(): lax.psum_scatter(part_rates, 'kv', scatter_dimension=0, tiled=True)  33.7 us
    all_gather x1, blocking collectives, local(): lax.all_gather(merged, 'kv', axis=0, tiled=True)  30.7 us
  transfers between devices with their start and end apart: 8, of which 8 were waited for; matrix products, arithmetic and copies ran while one was open for 1% of the time, Pallas kernels for 0%

profile of v1, /device:TPU:0, one launch (start us, length us, event | category | flops | bytes accessed | tf_op | source)
XLA Modules:
  0.0 629.0 jit_solution(8624223406759319436)
XLA Ops:
  7.3 6.9 %all_gather.12 = bf16[128,512]{1,0:T(8,128)(2,1)S(1)} all-gather(bf16[128,128]{1,0:T(8,128)(2,1)} %param.15), channel_id=1, replica_groups=mesh['kv'=8,'tp'=4] {'tp'}, dimensions={1}, use_global_device_ids=true | all-gather | bytes 163840 | tf_op jit(solution)/shard_map/all_gather | solution.py:48
  14.2 1.6 fusion.24
  15.8 1.7 fusion.22
  17.6 2.2 fusion.20
  19.8 1.7 fusion.18
  24.1 22.1 %all-reduce = f32[128]{0:T(128)S(1)} all-reduce(f32[128]{0:T(128)S(1)} %fusion.9), channel_id=4, replica_groups=mesh['kv'=8,'tp'=4] {'kv'}, use_global_device_ids=true, to_apply=%region_2.0.clone | all-reduce | flops 128 | bytes 1024
  46.3 33.7 %reduce-scatter.8.cloned.1.call-done = f32[16,48]{1,0:T(8,128)} async-done(((f32[128,48]{1,0:T(8,128)}), f32[16,48]{1,0:T(8,128)}) %reduce-scatter.8.cloned.1.call-update) | async-done | bytes 3088 | tf_op jit(solution)/shard_map/reduce_scatter | solution.py:63
  80.8 63.6 %reduce-scatter.10.cloned.1.call-done = f32[16,768]{1,0:T(8,128)} async-done(((f32[128,768]{1,0:T(8,128)}), f32[16,768]{1,0:T(8,128)}) %reduce-scatter.10.cloned.1.call-update) | async-done | bytes 49168 | tf_op jit(solution)/shard_map/reduce_scatter | solution.py:60
  144.4 64.5 %reduce-scatter.12.cloned.1.call-done = f32[16,768]{1,0:T(8,128)} async-done(((f32[128,768]{1,0:T(8,128)}), f32[16,768]{1,0:T(8,128)}) %reduce-scatter.12.cloned.1.call-update) | async-done | bytes 49168 | tf_op jit(solution)/shard_map/reduce_scatter | solution.py:61
  208.9 64.3 %reduce-scatter.14.cloned.1.call-done = f32[16,768]{1,0:T(8,128)} async-done(((f32[128,768]{1,0:T(8,128)}), f32[16,768]{1,0:T(8,128)}) %reduce-scatter.14.cloned.1.call-update) | async-done | bytes 49168 | tf_op jit(solution)/shard_map/reduce_scatter | solution.py:59
  273.3 64.9 %reduce-scatter.16.cloned.1.call-done = f32[16,768]{1,0:T(8,128)} async-done(((f32[128,768]{1,0:T(8,128)}), f32[16,768]{1,0:T(8,128)}) %reduce-scatter.16.cloned.1.call-update) | async-done | bytes 49168 | tf_op jit(solution)/shard_map/reduce_scatter | solution.py:62
  339.7 7.7 %fusion = f32[16,6,1,128]{3,2,1,0:T(1,128)S(1)} fusion(f32[16,6,128,128]{3,2,1,0:T(8,128)} %param.25, f32[16,6]{1,0:T(8,128)S(1)} %get-tuple-element.3, f32[16,6,128,1]{2,1,0,3:T(8,128)S(1)} %fusion.49), kind=kOutput, calls=%fused_computation.1 | convolution fusion | flops 20447232 | bytes 6390144 | tf_op jit(solution)/shard_map/bhkv,bhk->bhv/dot_general | solution.py:83
  347.6 4.5 multiply_add_fusion
  352.1 2.7 copy-done.1
  354.8 5.4 fusion.29
  360.4 30.7 %all_gather.13 = bf16[128,768]{1,0:T(8,128)(2,1)S(1)} all-gather(bf16[16,768]{1,0:T(8,128)(2,1)S(1)} %bitcast.47), channel_id=1, replica_groups=mesh['kv'=8,'tp'=4] {'kv'}, dimensions={0}, use_global_device_ids=true | all-gather | bytes 221184 | tf_op jit(solution)/shard_map/all_gather | solution.py:98
  392.2 19.2 %reduce-scatter.18.cloned.1.call-done = f32[128,128]{1,0:T(8,128)} async-done(((f32[128,512]{1,0:T(8,128)}), f32[128,128]{1,0:T(8,128)}) %reduce-scatter.18.cloned.1.call-update) | async-done | bytes 65552 | tf_op jit(solution)/shard_map/reduce_scatter | solution.py:100
  413.1 55.4 %all-gather.3.cloned.1.call-done = bf16[4096,128]{1,0:T(8,128)(2,1)} async-done(((bf16[128,128]{1,0:T(8,128)(2,1)}), bf16[4096,128]{1,0:T(8,128)(2,1)}) %all-gather.3.cloned.1.call-update) | async-done | bytes 1048592 | tf_op jit(solution)/shard_map/all_gather | solution.py:102
  468.5 1.5 multiply_reduce_fusion
  470.1 2.8 bitcast_convert_fusion
  472.9 1.9 copy.18
  474.8 1.7 fusion.4
  476.5 6.5 %fusion.7 = f32[128,4096]{1,0:T(8,128)} fusion(bf16[512,4096]{1,0:T(8,128)(2,1)} %param.29, bf16[128,4096]{0,1:T(8,128)(2,1)} %fusion.4, bf16[4096,512]{1,0:T(8,128)(2,1)} %param.28), kind=kOutput, calls=%fused_computation.11 | convolution fusion | flops 1073938432 | bytes 11534336 | tf_op jit(solution)/shard_map/dot_general | solution.py:24
  483.0 137.6 %reduce-scatter.20.cloned.1.call-done = f32[128,128]{1,0:T(8,128)} async-done(((f32[128,4096]{1,0:T(8,128)}), f32[128,128]{1,0:T(8,128)}) %reduce-scatter.20.cloned.1.call-update) | async-done | bytes 65552 | tf_op jit(solution)/shard_map/reduce_scatter | solution.py:104
  (67 shorter events, 9.0 us)
Async XLA Ops:
  7.2 8.6 %copy-start = (bf16[512,768]{1,0:T(8,128)(2,1)S(1)}, bf16[512,768]{1,0:T(8,128)(2,1)}, u32[]{:S(2)}) copy-start(bf16[512,768]{1,0:T(8,128)(2,1)} %param.18) | copy-start | bytes 2359300
  7.2 15.6 %copy-start.11 = (u32[32]{0:T(128)S(1)}, u32[32]{0:T(128)}, u32[]{:S(2)}) copy-start(u32[32]{0:T(128)} %constant.45) | copy-start | bytes 388
  7.2 14.4 %copy-start.7 = (f32[512]{0:T(512)S(1)}, f32[512]{0:T(512)}, u32[]{:S(2)}) copy-start(f32[512]{0:T(512)} %param.16) | copy-start | bytes 6148
  7.2 12.6 %copy-start.2 = (bf16[512,768]{1,0:T(8,128)(2,1)S(1)}, bf16[512,768]{1,0:T(8,128)(2,1)}, u32[]{:S(2)}) copy-start(bf16[512,768]{1,0:T(8,128)(2,1)} %param.17) | copy-start | bytes 2359300
  7.2 14.4 %copy-start.3 = (bf16[512,768]{1,0:T(8,128)(2,1)S(1)}, bf16[512,768]{1,0:T(8,128)(2,1)}, u32[]{:S(2)}) copy-start(bf16[512,768]{1,0:T(8,128)(2,1)} %param.20) | copy-start | bytes 2359300
  7.2 15.5 %copy-start.10 = (f32[6]{0:T(128)S(1)}, f32[6]{0:T(128)}, u32[]{:S(2)}) copy-start(f32[6]{0:T(128)} %param.23) | copy-start | bytes 76
  7.2 72.7 %reduce-scatter.8.cloned.1.call-start = ((), (), s32[]{:S(2)}) async-start(), calls=%async_computation.7 | async-start | bytes 73728 | tf_op jit(solution)/shard_map/reduce_scatter | solution.py:63
  15.8 128.7 %reduce-scatter.10.cloned.1.call-start = ((), (), s32[]{:S(2)}) async-start(), calls=%async_computation.8 | async-start | bytes 442368 | tf_op jit(solution)/shard_map/reduce_scatter | solution.py:60
  17.5 191.4 %reduce-scatter.12.cloned.1.call-start = ((), (), s32[]{:S(2)}) async-start(), calls=%async_computation.9 | async-start | bytes 442368 | tf_op jit(solution)/shard_map/reduce_scatter | solution.py:61
  19.8 253.5 %reduce-scatter.14.cloned.1.call-start = ((), (), s32[]{:S(2)}) async-start(), calls=%async_computation.10 | async-start | bytes 442368 | tf_op jit(solution)/shard_map/reduce_scatter | solution.py:59
  21.6 316.6 %reduce-scatter.16.cloned.1.call-start = ((), (), s32[]{:S(2)}) async-start(), calls=%async_computation.11 | async-start | bytes 442368 | tf_op jit(solution)/shard_map/reduce_scatter | solution.py:62
  22.7 388.7 %reduce-scatter.18.cloned.1.call-start = ((), (), s32[]{:S(2)}) async-start(), calls=%async_computation.12 | async-start | bytes 327680 | tf_op jit(solution)/shard_map/reduce_scatter | solution.py:100
  352.1 2.7 copy-start.1
  354.8 5.5 copy-start.9
  354.8 36.4 %copy-start.4 = (bf16[768,512]{1,0:T(8,128)(2,1)S(1)}, bf16[768,512]{1,0:T(8,128)(2,1)}, u32[]{:S(2)}) copy-start(bf16[768,512]{1,0:T(8,128)(2,1)} %param.26) | copy-start | bytes 2359300
  354.8 56.6 %copy-start.6 = (bf16[128,128]{1,0:T(8,128)(2,1)S(1)}, bf16[128,128]{1,0:T(8,128)(2,1)}, u32[]{:S(2)}) copy-start(bf16[128,128]{1,0:T(8,128)(2,1)} %param.15) | copy-start | bytes 98308
  392.1 76.4 %all-gather.3.cloned.1.call-start = ((), (), s32[]{:S(2)}) async-start(), calls=%async_computation.14 | async-start | bytes 1081344 | tf_op jit(solution)/shard_map/all_gather | solution.py:102
  412.9 207.7 %reduce-scatter.20.cloned.1.call-start = ((), (), s32[]{:S(2)}) async-start(), calls=%async_computation.13 | async-start | bytes 2162688 | tf_op jit(solution)/shard_map/reduce_scatter | solution.py:104
  468.5 6.3 %copy-start.8 = (f32[4096]{0:T(1024)S(1)}, f32[4096]{0:T(1024)}, u32[]{:S(2)}) copy-start(f32[4096]{0:T(1024)} %param.27) | copy-start | bytes 49156
  476.5 144.2 %copy-start.5 = (bf16[128,128]{1,0:T(8,128)(2,1)S(1)}, bf16[128,128]{1,0:T(8,128)(2,1)}, u32[]{:S(2)}) copy-start(bf16[128,128]{1,0:T(8,128)(2,1)} %add_convert_fusion.1) | copy-start | bytes 98308
Sparse Core Ops, SparseCore 0:
  15.9 64.0 reduce-scatter.7
  83.2 61.1 reduce-scatter.9
  147.7 61.1 reduce-scatter.11
  212.1 61.1 reduce-scatter.13
  277.0 61.2 reduce-scatter.15
  392.2 19.1 reduce-scatter.17
  414.9 53.6 all-gather.2
  483.2 137.4 reduce-scatter.19
